TPU v7x, 32 devices: a whole 2x2x4 slice. The times are simulated.
32 devices in a mesh: kv: 8 (over z, y), tp: 4 (over x, core).
Axes of the slice: x: 2, y: 2, z: 4, core: 2. Of those that a mesh axis runs over, the one named last changes fastest.
Arguments:
- tokens: bfloat16 [4, 4096], P(None, 'kv'), may hold values from -70 to 70
- norm_gain: float32 [4096], P('kv'), may hold values from 0.1 to 1.9
- query_weight: bfloat16 [4096, 2048], P('kv', 'tp'), may hold values from -0.09375 to 0.09375
- key_weight: bfloat16 [4096, 256], P('kv', 'tp'), may hold values from -0.09375 to 0.09375
- value_weight: bfloat16 [4096, 256], P('kv', 'tp'), may hold values from -0.09375 to 0.09375
- cache_keys: bfloat16 [4, 2, 6144, 128], P(None, None, ('kv', 'tp')), may hold values from -480 to 480, as said below
- cache_values: bfloat16 [4, 2, 6144, 128], P(None, None, ('kv', 'tp')), may hold values from -6 to 6
- lengths: int32 [4], replicated, may hold values from 1536 to 6143
- lambdas: float32 [16], P('tp'), may hold values from 0.3 to 0.8
- head_gain: float32 [128], replicated, may hold values from 0.1 to 1.9
- output_weight: bfloat16 [2048, 4096], P('tp', 'kv'), may hold values from -0.125 to 0.125
Outputs:
- attended: bfloat16 [4, 4096], P(None, 'kv')
- new_keys: bfloat16 [4, 256], P(None, 'tp')
- new_values: bfloat16 [4, 256], P(None, 'tp')
Inputs may be any that keep to these rules, and one draw needn't show every extreme that they name: `cache_keys`: of order 1.75 in most entries; some rows may be far larger.
All inputs are finite; a program needn't handle non-finite values.
Results may differ from a plain program's by a relative error of at most 0.038.
Values may be sent and summed in bfloat16 or wider, within the bound.
A program may use at most 64 MiB of HBM per device.

v0:
```python
import jax
import jax.numpy as jnp
from jax import lax
from jax.sharding import PartitionSpec as P

D = 4096
HEADS = 16
KV_HEADS = 2
QK = 64
VD = 128


NEG_FILL = -1e30


def body(
    tokens,
    norm_gain,
    query_weight,
    key_weight,
    value_weight,
    cache_keys,
    cache_values,
    lengths,
    lambdas,
    head_gain,
    output_weight,
):
    floats = tokens.astype(jnp.float32)
    scaled = (floats * norm_gain).astype(jnp.bfloat16)
    query_part = jnp.dot(scaled, query_weight, preferred_element_type=jnp.float32)
    key_part = jnp.dot(scaled, key_weight, preferred_element_type=jnp.float32)
    value_part = jnp.dot(scaled, value_weight, preferred_element_type=jnp.float32)
    squares, query_sum, key_sum, value_sum = lax.psum(
        (jnp.sum(floats * floats, axis=1), query_part, key_part, value_part), "kv"
    )
    inverse = lax.rsqrt(squares / D + 1e-06)[:, None]
    queries = (query_sum * inverse).astype(jnp.bfloat16)
    new_keys = (key_sum * inverse).astype(jnp.bfloat16)
    new_values = (value_sum * inverse).astype(jnp.bfloat16)
    every_query = lax.all_gather(queries, "tp", axis=1, tiled=True)
    seq_count = tokens.shape[0]
    pos_count = cache_keys.shape[2]
    group_size = HEADS // KV_HEADS
    own_heads = lambdas.shape[0]
    first_position = (lax.axis_index("kv") * lax.axis_size("tp") + lax.axis_index("tp")) * pos_count
    positions = first_position + jnp.arange(pos_count, dtype=jnp.int32)
    live_mask = (positions[None, :] < lengths[:, None])[:, None, None, None, :]
    query_rows = every_query.reshape(seq_count, KV_HEADS, group_size, 2, QK)
    key_rows = cache_keys.reshape(seq_count, KV_HEADS, pos_count, 2, QK)
    scores = jnp.einsum(
        "bhgcd,bhpcd->bhgcp", query_rows, key_rows, preferred_element_type=jnp.float32
    ) * QK ** (-0.5)
    scores = jnp.where(live_mask, scores, NEG_FILL)
    local_peak = jnp.max(scores, axis=-1)
    peak_used = lax.pmax(local_peak, ("kv", "tp"))
    weights = jnp.where(live_mask, jnp.exp(scores - peak_used[..., None]), 0.0)
    totals = jnp.sum(weights, axis=-1).reshape(seq_count, HEADS, 2)
    summed = jnp.einsum(
        "bhgcp,bhpv->bhgcv",
        weights.astype(jnp.bfloat16),
        cache_values,
        preferred_element_type=jnp.float32,
    ).reshape(seq_count, HEADS, 2, VD)
    totals, summed = (
        lax.psum_scatter(totals.astype(jnp.bfloat16), "tp", scatter_dimension=1, tiled=True).astype(
            jnp.float32
        ),
        lax.psum_scatter(summed.astype(jnp.bfloat16), "tp", scatter_dimension=1, tiled=True).astype(
            jnp.float32
        ),
    )
    totals, summed = lax.psum((totals, summed), "kv")
    ratios = summed / totals[..., None]
    mixed = ratios[:, :, 0] - lambdas[None, :, None] * ratios[:, :, 1]
    normed = mixed * lax.rsqrt(jnp.mean(mixed * mixed, axis=-1, keepdims=True) + 1e-06) * head_gain
    flattened = normed.astype(jnp.bfloat16).reshape(seq_count, own_heads * VD)
    partial_out = jnp.dot(flattened, output_weight, preferred_element_type=jnp.float32)
    attended = lax.psum(partial_out.astype(jnp.bfloat16), "tp")
    return (attended, new_keys, new_values)


def solution(mesh):
    return jax.shard_map(
        body,
        mesh=mesh,
        in_specs=(
            P(None, "kv"),
            P("kv"),
            P("kv", "tp"),
            P("kv", "tp"),
            P("kv", "tp"),
            P(None, None, ("kv", "tp"), None),
            P(None, None, ("kv", "tp"), None),
            P(),
            P("tp"),
            P(),
            P("tp", "kv"),
        ),
        out_specs=(P(None, "kv"), P(None, "tp"), P(None, "tp")),
        check_vma=False,
    )
```

profile of v0, /device:TPU:0, one launch (start us, length us, event | category | flops | bytes accessed | tf_op | source)
XLA Modules:
  0.0 127.6 jit_solution(1251713564693285807)
XLA Ops:
  0.6 0.0 copy-start
  0.7 0.8 broadcast_compare_fusion
  1.5 0.2 copy-done
  1.7 0.9 fusion.24
  2.6 0.1 fusion.11
  2.8 23.6 %all-reduce.3 = (f32[4,512]{1,0:T(4,128)S(1)}, f32[4]{0:T(128)S(1)}) all-reduce(f32[4,512]{1,0:T(4,128)S(1)} %fusion.24, f32[4]{0:T(128)S(1)} %fusion.11), channel_id=1, replica_groups=mesh['kv'=8,'tp'=4] {'kv'}, use_global_device_ids=true, to_apply=%region_0.0 | all-reduce | flops 2052 | bytes 16416 | tf_op jit(solution)/shard_map/psum | solution.py:34
  26.4 0.1 multiply_convert_fusion
  26.5 5.2 %all_gather.3 = bf16[4,2048]{1,0:T(4,128)(2,1)S(1)} all-gather(bf16[4,512]{1,0:T(4,128)(2,1)S(1)} %multiply_convert_fusion), channel_id=1, replica_groups=mesh['kv'=8,'tp'=4] {'tp'}, dimensions={1}, use_global_device_ids=true | all-gather | bytes 20480 | tf_op jit(solution)/shard_map/all_gather | solution.py:41
  31.7 0.1 reshape.63
  31.8 0.2 copy.22
  32.0 0.3 fusion.27
  32.3 36.9 %pmax.7 = f32[4,2,8,2]{2,3,1,0:T(2,128)S(1)} all-reduce(f32[4,2,8,2]{2,3,1,0:T(2,128)S(1)} %get-tuple-element.15), channel_id=1, replica_groups=mesh['kv'=8,'tp'=4] {'kv','tp'}, use_global_device_ids=true, to_apply=%region_4.0 | all-reduce | flops 128 | bytes 1024 | tf_op jit(solution)/shard_map/pmax | solution.py:56
  69.2 0.2 fusion.3
  69.4 0.1 convert_element_type.51
  69.5 0.3 convolution_convert_fusion
  69.8 0.0 copy-start.6
  69.8 11.5 %all-reduce.4 = (bf16[4,16,2,128]{3,1,2,0:T(8,128)(2,1)S(1)}, bf16[4,16,2]{1,2,0:T(2,128)(2,1)S(1)}) all-reduce(bf16[4,16,2,128]{3,1,2,0:T(8,128)(2,1)S(1)} %bitcast.69, bf16[4,16,2]{1,2,0:T(2,128)(2,1)S(1)} %convert_element_type.51), channel_id=2, replica_groups=mesh['kv'=8,'tp'=4] {'tp'}, use_global_device_ids=true, to_apply=%region_5.6.clone | all-reduce | flops 16512 | bytes 66048
  81.4 0.6 dynamic-slice
  82.6 0.1 dynamic-slice_convert_fusion.1
  82.7 0.1 fusion.20
  82.8 0.1 fusion.22
  83.0 35.9 %all-reduce.2 = (f32[4,4,2,128]{3,1,2,0:T(4,128)S(1)}, f32[4,4,2]{1,2,0:T(2,128)S(1)}, f32[4,64]{1,0:T(4,128)S(1)}, f32[4,64]{1,0:T(4,128)S(1)}) all-reduce(f32[4,4,2,128]{3,1,2,0:T(4,128)S(1)} %dynamic-slice_convert_fusion, f32[4,4,2]{1,2,0:T(2,128)S(1)} %dynamic-slice_convert_fusion.1, ...), channel_id=1, replica_groups=mesh['kv'=8,'tp'=4] {'kv'}, use_global_device_ids=true, to_apply=%region_6.7 | all-reduce | flops 4640 | bytes 37120 | tf_op jit(solution)/shard_map/psum | solution.py:73
  118.9 0.6 multiply_convert_fusion.1
  119.5 0.1 broadcast_divide_fusion
  119.6 0.0 copy-start.7
  119.7 0.6 copy-done.7
  120.3 0.2 fusion.16
  120.5 0.1 broadcast_bitcast_fusion
  120.5 0.6 copy-done.8
  121.1 0.1 broadcast_bitcast_fusion.1
  121.2 0.2 convolution_convert_fusion.1
  121.4 6.2 %psum.53 = bf16[4,512]{1,0:T(4,128)(2,1)} all-reduce(bf16[4,512]{1,0:T(4,128)(2,1)S(1)} %convolution_convert_fusion.1), channel_id=1, replica_groups=mesh['kv'=8,'tp'=4] {'tp'}, use_global_device_ids=true, to_apply=%region_11.12 | all-reduce | flops 2048 | bytes 8192 | tf_op jit(solution)/shard_map/psum | solution.py:79
  (23 shorter events, 0.1 us)
Async XLA Ops:
  0.6 1.1 copy-start
  0.6 31.1 %copy-start.2 = (bf16[4,2,192,128]{3,2,1,0:T(8,128)(2,1)S(1)}, bf16[4,2,192,128]{3,2,1,0:T(8,128)(2,1)}, u32[]{:S(2)}) copy-start(bf16[4,2,192,128]{3,2,1,0:T(8,128)(2,1)} %param.16) | copy-start | bytes 1179652
  1.7 0.9 copy-start.3
  32.0 37.5 %copy-start.9 = (bf16[4,2,192,128]{3,2,1,0:T(8,128)(2,1)S(1)}, bf16[4,2,192,128]{3,2,1,0:T(8,128)(2,1)}, u32[]{:S(2)}) copy-start(bf16[4,2,192,128]{3,2,1,0:T(8,128)(2,1)} %param.17) | copy-start | bytes 1179652
  69.5 51.7 %copy-start.1 = (bf16[512,512]{1,0:T(8,128)(2,1)S(1)}, bf16[512,512]{1,0:T(8,128)(2,1)}, u32[]{:S(2)}) copy-start(bf16[512,512]{1,0:T(8,128)(2,1)} %param.21) | copy-start | bytes 1572868
  69.7 11.6 %copy-start.10 = (u32[32]{0:T(128)S(1)}, u32[32]{0:T(128)}, u32[]{:S(2)}) copy-start(u32[32]{0:T(128)} %constant.32) | copy-start | bytes 388
  69.8 12.9 %copy-start.4 = (bf16[512,64]{0,1:T(8,128)(2,1)S(1)}, bf16[512,64]{0,1:T(8,128)(2,1)}, u32[]{:S(2)}) copy-start(bf16[512,64]{0,1:T(8,128)(2,1)} %param.15) | copy-start | bytes 196612
  69.8 12.9 %copy-start.6 = (f32[512]{0:T(512)S(1)}, f32[512]{0:T(512)}, u32[]{:S(2)}) copy-start(f32[512]{0:T(512)} %param.12) | copy-start | bytes 6148
  81.3 1.5 %copy-start.5 = (bf16[512,64]{0,1:T(8,128)(2,1)S(1)}, bf16[512,64]{0,1:T(8,128)(2,1)}, u32[]{:S(2)}) copy-start(bf16[512,64]{0,1:T(8,128)(2,1)} %param.14) | copy-start | bytes 196612
  119.6 0.7 copy-start.7
  120.5 0.7 copy-start.8
where the time goes:
time: 128 us
  blocking collectives  119 us (93%)
  local copies, waits for them, and re-layouts  2.65 us (2%)
  other arithmetic  2.17 us (2%)
  matrix products  1.87 us (1%)
  between operations  1.46 us (1%)
    pmax x1, blocking collectives, body(): peak_used = lax.pmax(local_peak, ('kv', 'tp'))  36.9 us
    psum x1, blocking collectives, body(): totals, summed = lax.psum((totals, summed), 'kv')  35.9 us
    psum x1, blocking collectives, body(): lax.psum((jnp.sum(floats * floats, axis=1), query_part, key_part, value_p...  23.6 us
    unnamed x1, blocking collectives  11.5 us
    psum x1, blocking collectives, body(): attended = lax.psum(partial_out.astype(jnp.bfloat16), 'tp')  6.24 us
    all_gather x1, blocking collectives, body(): every_query = lax.all_gather(queries, 'tp', axis=1, tiled=True)  5.19 us

commit v1 on v0

v1 whole, which is shorter than its diff:
```python
import functools

import jax
import jax.numpy as jnp
from jax import lax
from jax.experimental import pallas as pl
from jax.experimental.pallas import tpu as pltpu
from jax.sharding import PartitionSpec as P

MESH = pl.DeviceIdType.MESH
NEG_FILL = -1e30
LANES = 128
F32 = jnp.float32
BF16 = jnp.bfloat16


def kernel(
    dims,
    tokens,
    gain,
    query_weight,
    key_weight,
    value_weight,
    cache_keys,
    cache_values,
    lengths,
    lambdas,
    head_gain,
    output_weight,
    attended,
    new_keys,
    new_values,
    qw,
    kw,
    vw,
    ck,
    cv,
    ow,
    proj,
    qrows,
    qbuf,
    nsend,
    nbuf,
    abuf,
    nbuf2,
    abuf2,
    obuf,
    cols,
    load_sem,
    ps,
    pr,
    qs,
    qr,
    ns,
    nr,
    a_s,
    a_r,
    ns2,
    nr2,
    as2,
    ar2,
    os_,
    or_,
):
    n_kv, n_tp, width = dims
    seqs = tokens.shape[0]
    own_q = query_weight.shape[1]
    own_kv = key_weight.shape[1]
    heads = own_q // LANES
    kv_heads = cache_keys.shape[1]
    pos_count = cache_keys.shape[2]
    rows = 2 * heads * seqs
    tp_each = n_tp // kv_heads
    me_kv = lax.axis_index("kv")
    me_tp = lax.axis_index("tp")

    pairs = ((query_weight, qw), (key_weight, kw), (value_weight, vw),
             (cache_keys, ck), (cache_values, cv), (output_weight, ow))
    loads = [pltpu.make_async_copy(s, d, load_sem.at[i]) for i, (s, d) in enumerate(pairs)]
    for load in loads:
        load.start()

    kv_peers = [lax.rem(me_kv + d, n_kv) for d in range(1, n_kv)]
    tp_peers = [lax.rem(me_tp + d, n_tp) for d in range(1, n_tp)]

    barrier = pltpu.get_barrier_semaphore()
    for p in kv_peers:
        pl.semaphore_signal(barrier, inc=1, device_id=(p, me_tp), device_id_type=MESH)
    for p in tp_peers:
        pl.semaphore_signal(barrier, inc=1, device_id=(me_kv, p), device_id_type=MESH)

    def over_kv(buf, send, recv):
        return [
            pltpu.make_async_remote_copy(
                src_ref=buf.at[me_kv], dst_ref=buf.at[me_kv],
                send_sem=send.at[p], recv_sem=recv.at[me_kv],
                device_id=(p, me_tp), device_id_type=MESH,
            )
            for p in kv_peers
        ]

    def over_tp(buf, send, recv, source=None):
        return [
            pltpu.make_async_remote_copy(
                src_ref=buf.at[me_tp] if source is None else source.at[p],
                dst_ref=buf.at[me_tp],
                send_sem=send.at[p], recv_sem=recv.at[me_tp],
                device_id=(me_kv, p), device_id_type=MESH,
            )
            for p in tp_peers
        ]

    def arrived_kv(buf, send, recv):
        for p in kv_peers:
            pltpu.make_async_remote_copy(
                src_ref=buf.at[p], dst_ref=buf.at[p],
                send_sem=send.at[p], recv_sem=recv.at[p],
                device_id=(p, me_tp), device_id_type=MESH,
            ).wait_recv()

    def arrived_tp(buf, send, recv):
        for p in tp_peers:
            pltpu.make_async_remote_copy(
                src_ref=buf.at[p], dst_ref=buf.at[p],
                send_sem=send.at[p], recv_sem=recv.at[p],
                device_id=(me_kv, p), device_id_type=MESH,
            ).wait_recv()

    started = []

    def go(copies):
        for c in copies:
            c.start()
        started.extend(copies)

    floats = tokens[...].astype(F32)
    scaled = (floats * gain[...]).astype(BF16)
    squares = jnp.sum(floats * floats, axis=1, keepdims=True)
    high = squares.astype(BF16).astype(F32)
    lane4 = lax.broadcasted_iota(jnp.int32, (seqs, LANES), 1)
    proj[me_kv, :, proj.shape[2] - LANES:] = jnp.where(lane4 < 64, high, squares - high).astype(BF16)
    if own_q + 2 * own_kv < proj.shape[2] - LANES:
        gap = proj.shape[2] - LANES - own_q - 2 * own_kv
        proj[me_kv, :, own_q + 2 * own_kv:proj.shape[2] - LANES] = jnp.zeros((seqs, gap), BF16)
    for load in loads[:3]:
        load.wait()
    proj[me_kv, :, :own_q] = jnp.dot(scaled, qw[...], preferred_element_type=F32).astype(BF16)
    key_part = jnp.dot(scaled, kw[...], preferred_element_type=F32)
    value_part = jnp.dot(scaled, vw[...], preferred_element_type=F32)
    proj[me_kv, :, own_q:own_q + own_kv] = key_part.astype(BF16)
    proj[me_kv, :, own_q + own_kv:own_q + 2 * own_kv] = value_part.astype(BF16)
    pl.semaphore_wait(barrier, n_kv + n_tp - 2)
    go(over_kv(proj, ps, pr))

    half = rows * tp_each
    row_b = lax.rem(lax.broadcasted_iota(jnp.int32, (half, pos_count), 0), seqs)
    first = (me_kv * n_tp + me_tp) * pos_count
    position = first + lax.broadcasted_iota(jnp.int32, (half, pos_count), 1)
    limit = jnp.full((half, pos_count), lengths[0], jnp.int32)
    for b in range(1, seqs):
        limit = jnp.where(row_b == b, lengths[b], limit)
    live = position < limit
    lane_row = lax.broadcasted_iota(jnp.int32, (1, LANES), 1)
    within = lax.rem(lane_row, rows)
    factor = jnp.ones((1, LANES), F32)
    for j in range(heads):
        start = (heads + j) * seqs
        factor = jnp.where((within >= start) & (within < start + seqs), -lambdas[j], factor)

    arrived_kv(proj, ps, pr)
    total = proj[0].astype(F32)
    for k in range(1, n_kv):
        total = total + proj[k].astype(F32)
    base = total.shape[1] - LANES
    sq = total[:, base:base + 1] + total[:, base + 64:base + 65]
    inverse = lax.rsqrt(sq / width + 1e-06)
    for j in range(heads):
        qrows[j * seqs:(j + 1) * seqs, :] = total[:, j * LANES:(j + 1) * LANES] * inverse
    qbuf[me_tp] = qrows[...].astype(BF16)
    go(over_tp(qbuf, qs, qr))
    new_keys[...] = (total[:, own_q:own_q + own_kv] * inverse).astype(BF16)
    new_values[...] = (total[:, own_q + own_kv:own_q + 2 * own_kv] * inverse).astype(BF16)
    loads[3].wait()
    loads[4].wait()
    arrived_tp(qbuf, qs, qr)

    qlane = lax.broadcasted_iota(jnp.int32, (heads * seqs, LANES), 1)
    outs, peaks, sums = [], [], []
    for g in range(kv_heads):
        pieces = []
        for t in range(g * tp_each, (g + 1) * tp_each):
            q = qbuf[t].astype(F32) * 0.125
            pieces += [jnp.where(qlane < 64, q, 0.0), jnp.where(qlane >= 64, q, 0.0)]
        q_all = jnp.concatenate(pieces, axis=0).astype(BF16)
        scores = None
        for b in range(seqs):
            s = lax.dot_general(q_all, ck[b, g], (((1,), (1,)), ((), ())), preferred_element_type=F32)
            scores = s if b == 0 else jnp.where(row_b == b, s, scores)
        scores = jnp.where(live, scores, NEG_FILL)
        peak = jnp.max(scores, axis=1, keepdims=True)
        e = jnp.where(live, jnp.exp(scores - peak), 0.0)
        sums.append(jnp.sum(e, axis=1, keepdims=True))
        peaks.append(peak)
        acc = None
        for b in range(seqs):
            w = jnp.where(row_b == b, e, 0.0).astype(BF16)
            o = jnp.dot(w, cv[b, g], preferred_element_type=F32)
            acc = o if b == 0 else acc + o
        outs.append(acc)
    wide_lane = lax.broadcasted_iota(jnp.int32, (LANES, LANES), 1)
    peak_all = jnp.concatenate(peaks, axis=0)
    sum_all = jnp.concatenate(sums, axis=0)
    aux = jnp.where(wide_lane == 0, peak_all, jnp.where(wide_lane == 1, sum_all, 0.0)).T
    abuf[me_tp] = aux[0:2]
    go(over_tp(abuf, a_s, a_r))
    for g in range(kv_heads):
        for t in range(tp_each):
            nsend[g * tp_each + t] = outs[g][t * rows:(t + 1) * rows].astype(BF16)
    go(over_tp(nbuf, ns, nr, nsend))
    nbuf[me_tp] = nsend[me_tp]
    my_rows = pl.ds(pl.multiple_of(me_tp * rows, rows), rows)

    arrived_tp(abuf, a_s, a_r)
    m = [abuf[t, 0:1, :] for t in range(n_tp)]
    top = functools.reduce(jnp.maximum, m)
    scale = [jnp.exp(x - top) for x in m]
    denom = functools.reduce(jnp.add, [scale[t] * abuf[t, 1:2, :] for t in range(n_tp)])
    abuf2[me_kv, 0:1, :] = top
    abuf2[me_kv, 1:2, :] = denom
    go(over_kv(abuf2, as2, ar2))
    pad = [jnp.zeros((LANES - n_tp, LANES), F32)]
    cols[...] = jnp.concatenate(scale + pad, axis=0).T
    col = cols[my_rows, :]
    arrived_tp(nbuf, ns, nr)
    merged = functools.reduce(jnp.add, [col[:, t:t + 1] * nbuf[t].astype(F32) for t in range(n_tp)])
    nbuf2[me_kv] = merged.astype(BF16)
    go(over_kv(nbuf2, ns2, nr2))

    arrived_kv(abuf2, as2, ar2)
    m = [abuf2[k, 0:1, :] for k in range(n_kv)]
    top = functools.reduce(jnp.maximum, m)
    scale = [jnp.exp(x - top) for x in m]
    denom = functools.reduce(jnp.add, [scale[k] * abuf2[k, 1:2, :] for k in range(n_kv)])
    weight = factor / denom
    pad = [jnp.zeros((LANES - n_kv, LANES), F32)]
    cols[...] = jnp.concatenate([s * weight for s in scale] + pad, axis=0).T
    col = cols[my_rows, :]
    loads[5].wait()
    arrived_kv(nbuf2, ns2, nr2)
    ratio = functools.reduce(jnp.add, [col[:, k:k + 1] * nbuf2[k].astype(F32) for k in range(n_kv)])
    mixed = ratio[:rows // 2] + ratio[rows // 2:]
    normed = mixed * lax.rsqrt(jnp.mean(mixed * mixed, axis=1, keepdims=True) + 1e-06) * head_gain[...]
    qrows[...] = normed
    part = None
    for j in range(heads):
        x = qrows[j * seqs:(j + 1) * seqs, :].astype(BF16)
        o = jnp.dot(x, ow[j * LANES:(j + 1) * LANES, :], preferred_element_type=F32)
        part = o if j == 0 else part + o
    obuf[me_tp] = part.astype(BF16)
    go(over_tp(obuf, os_, or_))
    arrived_tp(obuf, os_, or_)
    out = obuf[0].astype(F32)
    for t in range(1, n_tp):
        out = out + obuf[t].astype(F32)
    attended[...] = out.astype(BF16)
    for c in started:
        c.wait_send()


def solution(mesh):
    n_kv, n_tp = mesh.shape["kv"], mesh.shape["tp"]

    def body(tokens, norm_gain, query_weight, key_weight, value_weight, cache_keys,
             cache_values, lengths, lambdas, head_gain, output_weight):
        seqs = tokens.shape[0]
        own_q = query_weight.shape[1]
        own_kv = key_weight.shape[1]
        heads = own_q // LANES
        rows = 2 * heads * seqs
        out_cols = output_weight.shape[1]
        side = -(-2 * own_kv // LANES) * LANES
        any_ = pl.BlockSpec(memory_space=pl.ANY)
        vmem = pl.BlockSpec(memory_space=pltpu.VMEM)
        smem = pl.BlockSpec(memory_space=pltpu.SMEM)
        dma = pltpu.SemaphoreType.DMA
        return pl.pallas_call(
            functools.partial(kernel, (n_kv, n_tp, tokens.shape[1] * n_kv)),
            out_shape=(
                jax.ShapeDtypeStruct((seqs, out_cols), BF16),
                jax.ShapeDtypeStruct((seqs, own_kv), BF16),
                jax.ShapeDtypeStruct((seqs, own_kv), BF16),
            ),
            in_specs=[vmem, vmem, any_, any_, any_, any_, any_, smem, smem, vmem, any_],
            out_specs=(vmem, vmem, vmem),
            scratch_shapes=[
                pltpu.VMEM(query_weight.shape, BF16),
                pltpu.VMEM(key_weight.shape, BF16),
                pltpu.VMEM(value_weight.shape, BF16),
                pltpu.VMEM(cache_keys.shape, BF16),
                pltpu.VMEM(cache_values.shape, BF16),
                pltpu.VMEM(output_weight.shape, BF16),
                pltpu.VMEM((n_kv, seqs, own_q + side + LANES), BF16),
                pltpu.VMEM((heads * seqs, LANES), F32),
                pltpu.VMEM((n_tp, heads * seqs, LANES), BF16),
                pltpu.VMEM((n_tp, rows, LANES), BF16),
                pltpu.VMEM((n_tp, rows, LANES), BF16),
                pltpu.VMEM((n_tp, 2, LANES), F32),
                pltpu.VMEM((n_kv, rows, LANES), BF16),
                pltpu.VMEM((n_kv, 2, LANES), F32),
                pltpu.VMEM((n_tp, seqs, out_cols), BF16),
                pltpu.VMEM((LANES, LANES), F32),
                dma((6,)),
                dma((n_kv,)), dma((n_kv,)),
                dma((n_tp,)), dma((n_tp,)),
                dma((n_tp,)), dma((n_tp,)),
                dma((n_tp,)), dma((n_tp,)),
                dma((n_kv,)), dma((n_kv,)),
                dma((n_kv,)), dma((n_kv,)),
                dma((n_tp,)), dma((n_tp,)),
            ],
            compiler_params=pltpu.CompilerParams(collective_id=0, has_side_effects=True),
        )(tokens, norm_gain[None, :], query_weight, key_weight, value_weight, cache_keys,
          cache_values, lengths, lambdas, head_gain[None, :], output_weight)

    return jax.shard_map(
        body,
        mesh=mesh,
        in_specs=(
            P(None, "kv"),
            P("kv"),
            P("kv", "tp"),
            P("kv", "tp"),
            P("kv", "tp"),
            P(None, None, ("kv", "tp"), None),
            P(None, None, ("kv", "tp"), None),
            P(),
            P("tp"),
            P(),
            P("tp", "kv"),
        ),
        out_specs=(P(None, "kv"), P(None, "tp"), P(None, "tp")),
        check_vma=False,
    )
```

time: 128 us -> 32.4 us (0.25)
  blocking collectives: 119 us -> 0 us
  Pallas kernels: 0 us -> 26.6 us
  local copies, waits for them, and re-layouts: 2.65 us -> 4.89 us
  other arithmetic: 2.17 us -> 0 us
  matrix products: 1.87 us -> 0 us
    psum x3 -> x0, blocking collectives: 65.8 us -> none  [the longest x1 35.9 us: body(): totals, summed = lax.psum((totals, summed), 'kv')]
    pmax x1 -> x0, blocking collectives: 36.9 us -> none  [body(): peak_used = lax.pmax(local_peak, ('kv', 'tp'))]
    pallas_call x0 -> x1, Pallas kernels: none -> 26.6 us  [body(): pl.pallas_call(functools.partial(kernel, (n_kv, n_tp, tokens.shape[1] * n...]
    unnamed x1 -> x0, blocking collectives: 11.5 us -> none
    all_gather x1 -> x0, blocking collectives: 5.19 us -> none  [body(): every_query = lax.all_gather(queries, 'tp', axis=1, tiled=True)]
    unnamed x26 -> x13, local copies, waits for them, and re-layouts: 2.37 us -> 4.89 us
    dot_general x6 -> x0, matrix products: 1.87 us -> none  [the longest x1 0.93 us: body(): jnp.dot(scaled, query_weight, preferred_element_type=jnp.float32)]
where the time goes in v1:
time: 32.4 us; the launch traced here: 32.1 us
  Pallas kernels  26.6 us (82%)
  local copies, waits for them, and re-layouts  4.89 us (15%)
  between operations  0.66 us (2%)
    pallas_call x1, Pallas kernels, body(): pl.pallas_call(functools.partial(kernel, (n_kv, n_tp, tokens.shape[1] * n...  26.6 us
    unnamed x13, local copies, waits for them, and re-layouts  4.89 us

profile of v1, /device:TPU:0, one launch (start us, length us, event | category | flops | bytes accessed | tf_op | source)
XLA Modules:
  0.0 32.1 jit_solution(2820550512072790762)
XLA Ops:
  0.6 0.0 copy-start
  0.6 1.6 %copy.14.key_weight = bf16[512,64]{1,0:T(8,128)(2,1)} copy(bf16[512,64]{0,1:T(8,128)(2,1)} %param.14) | data formatting | bytes 131072 | tf_op args[3]
  2.3 0.0 copy-done
  2.3 0.8 %copy.15.value_weight = bf16[512,64]{1,0:T(8,128)(2,1)} copy(bf16[512,64]{0,1:T(8,128)(2,1)S(1)} %copy-done) | data formatting | bytes 131072 | tf_op args[4]
  3.0 26.6 %shard_map.130 = (bf16[4,512]{1,0:T(4,128)(2,1)}, bf16[4,64]{1,0:T(4,128)(2,1)}, bf16[4,64]{1,0:T(4,128)(2,1)}) custom-call(bf16[4,512]{1,0:T(4,128)(2,1)} %tokens.1, f32[1,512]{1,0:T(1,128)} %bitcast.2, bf16[512,512]{1,0:T(8,128)(2,1)} %query_weight.1, bf16[512,64]{1,0:T(8,128)(2,1)} %copy.14.key_weight, bf16[512,64]{1,0:T(8,128)(2,1)} %copy.15.value_weight, ...), custom_call_target="tpu_custom_call" | custom-call | tf_op jit(solution)/shard_map/pallas_call | solution.py:286
  29.6 0.0 copy-start.1
  29.6 0.7 %copy-done.1 = bf16[4,512]{1,0:T(4,128)(2,1)S(1)} copy-done((bf16[4,512]{1,0:T(4,128)(2,1)S(1)}, bf16[4,512]{1,0:T(4,128)(2,1)}, u32[]{:S(2)}) %copy-start.1) | copy-done | bytes 4120
  30.3 0.0 copy-start.3
  30.3 0.6 %copy.19 = bf16[4,512]{1,0:T(4,128)(2,1)} copy(bf16[4,512]{1,0:T(4,128)(2,1)S(1)} %copy-done.1) | data formatting | bytes 8192
  30.9 0.0 copy-done.3
  30.9 0.0 copy-start.2
  30.9 0.6 %copy.20 = bf16[4,64]{1,0:T(4,128)(2,1)} copy(bf16[4,64]{1,0:T(4,128)(2,1)S(1)} %copy-done.3) | data formatting | bytes 1024
  31.5 0.1 copy-done.2
  31.6 0.6 %copy.21 = bf16[4,64]{1,0:T(4,128)(2,1)} copy(bf16[4,64]{1,0:T(4,128)(2,1)S(1)} %copy-done.2) | data formatting | bytes 1024
Async XLA Ops:
  0.6 1.6 %copy-start = (bf16[512,64]{0,1:T(8,128)(2,1)S(1)}, bf16[512,64]{0,1:T(8,128)(2,1)}, u32[]{:S(2)}) copy-start(bf16[512,64]{0,1:T(8,128)(2,1)} %param.15) | copy-start | bytes 196612
  29.6 0.7 %copy-start.1 = (bf16[4,512]{1,0:T(4,128)(2,1)S(1)}, bf16[4,512]{1,0:T(4,128)(2,1)}, u32[]{:S(2)}) copy-start(bf16[4,512]{1,0:T(4,128)(2,1)} %get-tuple-element.6) | copy-start | bytes 12292
  30.3 0.6 %copy-start.3 = (bf16[4,64]{1,0:T(4,128)(2,1)S(1)}, bf16[4,64]{1,0:T(4,128)(2,1)}, u32[]{:S(2)}) copy-start(bf16[4,64]{1,0:T(4,128)(2,1)} %get-tuple-element.7) | copy-start | bytes 1540
  30.9 0.6 %copy-start.2 = (bf16[4,64]{1,0:T(4,128)(2,1)S(1)}, bf16[4,64]{1,0:T(4,128)(2,1)}, u32[]{:S(2)}) copy-start(bf16[4,64]{1,0:T(4,128)(2,1)} %get-tuple-element.8) | copy-start | bytes 1540

commit v2 on v1

--- a/solution.py
+++ b/solution.py
@@ -16,20 +16,23 @@
 
 def kernel(
     dims,
-    tokens,
-    gain,
+    tokens_in,
+    gain_in,
     query_weight,
     key_weight,
     value_weight,
     cache_keys,
     cache_values,
+    lengths_in,
+    lambdas_in,
+    head_gain_in,
+    output_weight,
+    packed,
+    tokens,
+    gain,
     lengths,
     lambdas,
     head_gain,
-    output_weight,
-    attended,
-    new_keys,
-    new_values,
     qw,
     kw,
     vw,
@@ -65,7 +68,8 @@
     n_kv, n_tp, width = dims
     seqs = tokens.shape[0]
     own_q = query_weight.shape[1]
-    own_kv = key_weight.shape[1]
+    own_kv = key_weight.shape[0]
+    out_cols = output_weight.shape[1]
     heads = own_q // LANES
     kv_heads = cache_keys.shape[1]
     pos_count = cache_keys.shape[2]
@@ -74,12 +78,6 @@
     me_kv = lax.axis_index("kv")
     me_tp = lax.axis_index("tp")
 
-    pairs = ((query_weight, qw), (key_weight, kw), (value_weight, vw),
-             (cache_keys, ck), (cache_values, cv), (output_weight, ow))
-    loads = [pltpu.make_async_copy(s, d, load_sem.at[i]) for i, (s, d) in enumerate(pairs)]
-    for load in loads:
-        load.start()
-
     kv_peers = [lax.rem(me_kv + d, n_kv) for d in range(1, n_kv)]
     tp_peers = [lax.rem(me_tp + d, n_tp) for d in range(1, n_tp)]
 
@@ -88,6 +86,13 @@
         pl.semaphore_signal(barrier, inc=1, device_id=(p, me_tp), device_id_type=MESH)
     for p in tp_peers:
         pl.semaphore_signal(barrier, inc=1, device_id=(me_kv, p), device_id_type=MESH)
+
+    pairs = ((tokens_in, tokens), (gain_in, gain), (query_weight, qw), (key_weight, kw),
+             (value_weight, vw), (lengths_in, lengths), (lambdas_in, lambdas),
+             (head_gain_in, head_gain), (cache_keys, ck), (cache_values, cv), (output_weight, ow))
+    loads = [pltpu.make_async_copy(s, d, load_sem.at[i]) for i, (s, d) in enumerate(pairs)]
+    for load in loads:
+        load.start()
 
     def over_kv(buf, send, recv):
         return [
@@ -133,6 +138,8 @@
             c.start()
         started.extend(copies)
 
+    for load in loads[:2]:
+        load.wait()
     floats = tokens[...].astype(F32)
     scaled = (floats * gain[...]).astype(BF16)
     squares = jnp.sum(floats * floats, axis=1, keepdims=True)
@@ -142,16 +149,18 @@
     if own_q + 2 * own_kv < proj.shape[2] - LANES:
         gap = proj.shape[2] - LANES - own_q - 2 * own_kv
         proj[me_kv, :, own_q + 2 * own_kv:proj.shape[2] - LANES] = jnp.zeros((seqs, gap), BF16)
-    for load in loads[:3]:
+    for load in loads[2:5]:
         load.wait()
     proj[me_kv, :, :own_q] = jnp.dot(scaled, qw[...], preferred_element_type=F32).astype(BF16)
-    key_part = jnp.dot(scaled, kw[...], preferred_element_type=F32)
-    value_part = jnp.dot(scaled, vw[...], preferred_element_type=F32)
+    key_part = lax.dot_general(scaled, kw[...], (((1,), (1,)), ((), ())), preferred_element_type=F32)
+    value_part = lax.dot_general(scaled, vw[...], (((1,), (1,)), ((), ())), preferred_element_type=F32)
     proj[me_kv, :, own_q:own_q + own_kv] = key_part.astype(BF16)
     proj[me_kv, :, own_q + own_kv:own_q + 2 * own_kv] = value_part.astype(BF16)
     pl.semaphore_wait(barrier, n_kv + n_tp - 2)
     go(over_kv(proj, ps, pr))
 
+    for load in loads[5:8]:
+        load.wait()
     half = rows * tp_each
     row_b = lax.rem(lax.broadcasted_iota(jnp.int32, (half, pos_count), 0), seqs)
     first = (me_kv * n_tp + me_tp) * pos_count
@@ -178,10 +187,9 @@
         qrows[j * seqs:(j + 1) * seqs, :] = total[:, j * LANES:(j + 1) * LANES] * inverse
     qbuf[me_tp] = qrows[...].astype(BF16)
     go(over_tp(qbuf, qs, qr))
-    new_keys[...] = (total[:, own_q:own_q + own_kv] * inverse).astype(BF16)
-    new_values[...] = (total[:, own_q + own_kv:own_q + 2 * own_kv] * inverse).astype(BF16)
-    loads[3].wait()
-    loads[4].wait()
+    packed[:, out_cols:] = (total[:, own_q:own_q + 2 * own_kv] * inverse).astype(BF16)
+    loads[8].wait()
+    loads[9].wait()
     arrived_tp(qbuf, qs, qr)
 
     qlane = lax.broadcasted_iota(jnp.int32, (heads * seqs, LANES), 1)
@@ -245,7 +253,7 @@
     pad = [jnp.zeros((LANES - n_kv, LANES), F32)]
     cols[...] = jnp.concatenate([s * weight for s in scale] + pad, axis=0).T
     col = cols[my_rows, :]
-    loads[5].wait()
+    loads[10].wait()
     arrived_kv(nbuf2, ns2, nr2)
     ratio = functools.reduce(jnp.add, [col[:, k:k + 1] * nbuf2[k].astype(F32) for k in range(n_kv)])
     mixed = ratio[:rows // 2] + ratio[rows // 2:]
@@ -262,9 +270,17 @@
     out = obuf[0].astype(F32)
     for t in range(1, n_tp):
         out = out + obuf[t].astype(F32)
-    attended[...] = out.astype(BF16)
+    packed[:, :out_cols] = out.astype(BF16)
     for c in started:
         c.wait_send()
+
+
+def split(packed, attended, new_keys, new_values):
+    cols, own = attended.shape[1], new_keys.shape[1]
+    attended[...] = packed[:, :cols]
+    rest = packed[:, cols:].astype(F32)
+    new_keys[...] = rest[:, :own].astype(BF16)
+    new_values[...] = rest[:, own:].astype(BF16)
 
 
 def solution(mesh):
@@ -281,21 +297,21 @@
         side = -(-2 * own_kv // LANES) * LANES
         any_ = pl.BlockSpec(memory_space=pl.ANY)
         vmem = pl.BlockSpec(memory_space=pltpu.VMEM)
-        smem = pl.BlockSpec(memory_space=pltpu.SMEM)
         dma = pltpu.SemaphoreType.DMA
-        return pl.pallas_call(
+        packed = pl.pallas_call(
             functools.partial(kernel, (n_kv, n_tp, tokens.shape[1] * n_kv)),
-            out_shape=(
-                jax.ShapeDtypeStruct((seqs, out_cols), BF16),
-                jax.ShapeDtypeStruct((seqs, own_kv), BF16),
-                jax.ShapeDtypeStruct((seqs, own_kv), BF16),
-            ),
-            in_specs=[vmem, vmem, any_, any_, any_, any_, any_, smem, smem, vmem, any_],
-            out_specs=(vmem, vmem, vmem),
+            out_shape=jax.ShapeDtypeStruct((seqs, out_cols + 2 * own_kv), BF16),
+            in_specs=[any_] * 11,
+            out_specs=vmem,
             scratch_shapes=[
+                pltpu.VMEM(tokens.shape, BF16),
+                pltpu.VMEM((1, tokens.shape[1]), F32),
+                pltpu.SMEM(lengths.shape, jnp.int32),
+                pltpu.SMEM(lambdas.shape, F32),
+                pltpu.VMEM((1, LANES), F32),
                 pltpu.VMEM(query_weight.shape, BF16),
-                pltpu.VMEM(key_weight.shape, BF16),
-                pltpu.VMEM(value_weight.shape, BF16),
+                pltpu.VMEM(key_weight.shape[::-1], BF16),
+                pltpu.VMEM(value_weight.shape[::-1], BF16),
                 pltpu.VMEM(cache_keys.shape, BF16),
                 pltpu.VMEM(cache_values.shape, BF16),
                 pltpu.VMEM(output_weight.shape, BF16),
@@ -309,7 +325,7 @@
                 pltpu.VMEM((n_kv, 2, LANES), F32),
                 pltpu.VMEM((n_tp, seqs, out_cols), BF16),
                 pltpu.VMEM((LANES, LANES), F32),
-                dma((6,)),
+                dma((11,)),
                 dma((n_kv,)), dma((n_kv,)),
                 dma((n_tp,)), dma((n_tp,)),
                 dma((n_tp,)), dma((n_tp,)),
@@ -319,8 +335,18 @@
                 dma((n_tp,)), dma((n_tp,)),
             ],
             compiler_params=pltpu.CompilerParams(collective_id=0, has_side_effects=True),
-        )(tokens, norm_gain[None, :], query_weight, key_weight, value_weight, cache_keys,
+        )(tokens, norm_gain[None, :], query_weight, key_weight.T, value_weight.T, cache_keys,
           cache_values, lengths, lambdas, head_gain[None, :], output_weight)
+        return pl.pallas_call(
+            split,
+            out_shape=(
+                jax.ShapeDtypeStruct((seqs, out_cols), BF16),
+                jax.ShapeDtypeStruct((seqs, own_kv), BF16),
+                jax.ShapeDtypeStruct((seqs, own_kv), BF16),
+            ),
+            in_specs=[vmem],
+            out_specs=(vmem, vmem, vmem),
+        )(packed)
 
     return jax.shard_map(
         body,

time: 32.4 us -> 28 us (0.86)
  local copies, waits for them, and re-layouts: 4.89 us -> 0 us
  Pallas kernels: 26.6 us -> 27.1 us
    unnamed x13 -> x0, local copies, waits for them, and re-layouts: 4.89 us -> none
    pallas_call x0 -> x1, Pallas kernels: none -> 1.33 us  [body(): pl.pallas_call(split, out_shape=(jax.ShapeDtypeStruct((seqs, out_cols), B...]
    pallas_call x1, Pallas kernels: 26.6 us -> 25.8 us  [body(): pl.pallas_call(functools.partial(kernel, (n_kv, n_tp, tokens.shape[1] * n...]
where the time goes in v2:
time: 28 us; the launch traced here: 27.8 us
  Pallas kernels  27.1 us (97%)
  between operations  0.64 us (2%)
    pallas_call x1, Pallas kernels, body(): pl.pallas_call(functools.partial(kernel, (n_kv, n_tp, tokens.shape[1] * n...  25.8 us
    pallas_call x1, Pallas kernels, body(): pl.pallas_call(split, out_shape=(jax.ShapeDtypeStruct((seqs, out_cols), B...  1.33 us

profile of v2, /device:TPU:0, one launch (start us, length us, event | category | flops | bytes accessed | tf_op | source)
XLA Modules:
  0.0 27.8 jit_solution(5395172086535219150)
XLA Ops:
  0.6 25.8 %shard_map.130.packed = bf16[4,640]{1,0:T(4,128)(2,1)} custom-call(bf16[4,512]{1,0:T(4,128)(2,1)} %tokens_in.1, f32[1,512]{1,0:T(1,128)} %bitcast.6, bf16[512,512]{1,0:T(8,128)(2,1)} %query_weight.1, bf16[64,512]{1,0:T(8,128)(2,1)} %bitcast.4, bf16[64,512]{1,0:T(8,128)(2,1)} %bitcast.5, bf16[4,2,192,128]{3,2,1,0:T(8,128)(2,1)} %cache_keys.1, ...), custom_call_target="tpu_custom_call" | custom-call | tf_op jit(solution)/shard_map/pallas_call | solution.py:301
  26.5 1.3 %shard_map.131 = (bf16[4,512]{1,0:T(4,128)(2,1)}, bf16[4,64]{1,0:T(4,128)(2,1)}, bf16[4,64]{1,0:T(4,128)(2,1)}) custom-call(bf16[4,640]{1,0:T(4,128)(2,1)} %shard_map.130.packed), custom_call_target="tpu_custom_call" | custom-call | tf_op jit(solution)/shard_map/pallas_call | solution.py:340

commit v3 on v2

--- a/solution.py
+++ b/solution.py
@@ -12,6 +12,14 @@
 LANES = 128
 F32 = jnp.float32
 BF16 = jnp.bfloat16
+
+
+def far_first(me, n):
+    if n & (n - 1):
+        return [lax.rem(me + d, n) for d in range(1, n)]
+    bits = [1 << i for i in range(n.bit_length() - 1)]
+    flips = {bit: bit * (1 - 2 * lax.rem(me // bit, 2)) for bit in bits}
+    return [me + sum(flips[bit] for bit in bits if d & bit) for d in range(n - 1, 0, -1)]
 
 
 def kernel(
@@ -78,8 +86,8 @@
     me_kv = lax.axis_index("kv")
     me_tp = lax.axis_index("tp")
 
-    kv_peers = [lax.rem(me_kv + d, n_kv) for d in range(1, n_kv)]
-    tp_peers = [lax.rem(me_tp + d, n_tp) for d in range(1, n_tp)]
+    kv_peers = far_first(me_kv, n_kv)
+    tp_peers = far_first(me_tp, n_tp)
 
     barrier = pltpu.get_barrier_semaphore()
     for p in kv_peers:
@@ -300,7 +308,7 @@
         dma = pltpu.SemaphoreType.DMA
         packed = pl.pallas_call(
             functools.partial(kernel, (n_kv, n_tp, tokens.shape[1] * n_kv)),
-            out_shape=jax.ShapeDtypeStruct((seqs, out_cols + 2 * own_kv), BF16),
+            out_shape=pltpu.VMEM((seqs, out_cols + 2 * own_kv), BF16),
             in_specs=[any_] * 11,
             out_specs=vmem,
             scratch_shapes=[
@@ -346,7 +354,7 @@
             ),
             in_specs=[vmem],
             out_specs=(vmem, vmem, vmem),
-        )(packed)
+        )(pltpu.with_memory_space_constraint(packed, pltpu.VMEM))
 
     return jax.shard_map(
         body,

time: 28 us -> 26.5 us (0.946)
  Pallas kernels: 27.1 us -> 25.7 us
    pallas_call x1, Pallas kernels: 25.8 us -> 25 us  [body(): pl.pallas_call(functools.partial(kernel, (n_kv, n_tp, tokens.shape[1] * n...]
    pallas_call x1, Pallas kernels: 1.33 us -> 0.64 us  [body(): pl.pallas_call(split, out_shape=(jax.ShapeDtypeStruct((seqs, out_cols), B...]
where the time goes in v3:
time: 26.5 us; the launch traced here: 26.3 us
  Pallas kernels  25.7 us (97%)
  between operations  0.64 us (2%)
    pallas_call x1, Pallas kernels, body(): pl.pallas_call(functools.partial(kernel, (n_kv, n_tp, tokens.shape[1] * n...  25 us
    pallas_call x1, Pallas kernels, body(): pl.pallas_call(split, out_shape=(jax.ShapeDtypeStruct((seqs, out_cols), B...  0.64 us

profile of v3, /device:TPU:0, one launch (start us, length us, event | category | flops | bytes accessed | tf_op | source)
XLA Modules:
  0.0 26.3 jit_solution(6411157425080012125)
XLA Ops:
  0.6 25.0 %shard_map.130.packed = bf16[4,640]{1,0:T(4,128)(2,1)S(1)} custom-call(bf16[4,512]{1,0:T(4,128)(2,1)} %tokens_in.1, f32[1,512]{1,0:T(1,128)} %bitcast.6, bf16[512,512]{1,0:T(8,128)(2,1)} %query_weight.1, bf16[64,512]{1,0:T(8,128)(2,1)} %bitcast.4, bf16[64,512]{1,0:T(8,128)(2,1)} %bitcast.5, bf16[4,2,192,128]{3,2,1,0:T(8,128)(2,1)} %cache_keys.1, ...), custom_call_target="tpu_custom_call" | custom-call | tf_op jit(solution)/shard_map/pallas_call | solution.py:309
  25.7 0.6 %shard_map.131 = (bf16[4,512]{1,0:T(4,128)(2,1)}, bf16[4,64]{1,0:T(4,128)(2,1)}, bf16[4,64]{1,0:T(4,128)(2,1)}) custom-call(bf16[4,640]{1,0:T(4,128)(2,1)S(1)} %shard_map.130.packed), custom_call_target="tpu_custom_call" | custom-call | tf_op jit(solution)/shard_map/pallas_call | solution.py:348
